TPU v7x, 32 devices: a whole 2x2x4 slice. The times are simulated.
32 devices in a mesh: sp: 8 (over z, x), tp: 4 (over y, core).
Axes of the slice: x: 2, y: 2, z: 4, core: 2. Of those that a mesh axis runs over, the one named last changes fastest.
Arguments:
- pool_input: bfloat16 [1024, 1024], P('sp', 'tp'), may hold values from -12 to 12
- doc_ids: int32 [1024], P('sp'), may hold values from 0 to 1, as said below
- residual: bfloat16 [1024, 2048], P('sp', 'tp'), may hold values from -30 to 30
- pool_gain: float32 [1024], P('tp'), may hold values from 0.1 to 1.9
- out_proj: bfloat16 [1024, 2048], P('tp'), may hold values from -0.25 to 0.25
- norm_gain: float32 [2048], P('tp'), may hold values from 0.1 to 1.9
- routes: int32 [1024, 2], P('sp'), may hold values from 0 to 7, all different within a row; in each aligned block of 128 rows (0 to 127, 128 to 255, ...) at most 64 rows name the same one
- route_weights: float32 [1024, 2], P('sp'), may hold values from 0.2 to 1.2
- expert_gate: bfloat16 [8, 2048, 4096], P('sp', None, 'tp'), may hold values from -0.125 to 0.125
- expert_up: bfloat16 [8, 2048, 4096], P('sp', None, 'tp'), may hold values from -0.125 to 0.125
- expert_down: bfloat16 [8, 4096, 2048], P('sp', 'tp'), may hold values from -0.125 to 0.125
- shared_gate: bfloat16 [2048, 1024], P(None, 'tp'), may hold values from -0.125 to 0.125
- shared_up: bfloat16 [2048, 1024], P(None, 'tp'), may hold values from -0.125 to 0.125
- shared_down: bfloat16 [1024, 2048], P('tp'), may hold values from -0.25 to 0.25
Outputs:
- layer_out: bfloat16 [1024, 2048], P('sp', 'tp')
Inputs may be any that keep to these rules, and one draw needn't show every extreme that they name: `routes`: each row names 2 different experts. In each aligned block of 128 rows no expert is named by more than 64 rows; in some blocks one expert is named by exactly 64 rows. `doc_ids`: document numbers start at 0, never fall along the sequence and rise by one at each document's start.
All inputs are finite; a program needn't handle non-finite values.
Results may differ from a plain program's by a relative error of at most 0.015.
Values may be sent and summed in bfloat16 or wider, within the bound.
A program may use at most 64 MiB of HBM per device.

v0:
```python
import jax
import functools
import jax.numpy as jnp
from jax import lax
from jax.experimental import pallas as pl
from jax.experimental.pallas import tpu as pltpu
from jax.sharding import PartitionSpec as P


def carried_in(value, axis, join, neutral):
    count, mine = (lax.axis_size(axis), lax.axis_index(axis))
    pieces = jax.tree.map(lambda part: lax.all_gather(part, axis), value)
    subtotal = jax.tree.map(
        lambda part, zero: jnp.full_like(part, 0) + jnp.asarray(zero, part.dtype), value, neutral
    )

    def hop(position, subtotal):
        longer = join(subtotal, jax.tree.map(lambda part: part[position], pieces))
        return jax.tree.map(lambda new, old: jnp.where(position < mine, new, old), longer, subtotal)

    return lax.fori_loop(0, count - 1, hop, subtotal)


def from_behind(value, axis, by):
    size = lax.axis_size(axis)
    pairs = [(i, i + by) for i in range(size) if 0 <= i + by < size]
    return lax.ppermute(value, axis, pairs)


def join_documents(earlier, later):
    earlier_sum, earlier_length, earlier_first, earlier_last, earlier_inner = earlier
    later_sum, later_length, later_first, later_last, later_inner = later
    boundary = later_first != earlier_last
    restart = (later_inner > 0) | boundary
    merged = (
        jnp.where(restart, later_sum, earlier_sum + later_sum),
        jnp.where(restart, later_length, earlier_length + later_length),
        earlier_first,
        later_last,
        jnp.maximum(jnp.maximum(earlier_inner, later_inner), boundary.astype(jnp.float32)),
    )
    earlier_empty = earlier_first < 0
    later_empty = later_first < 0
    return tuple(
        (
            jnp.where(earlier_empty, second, jnp.where(later_empty, first_value, joined))
            for first_value, second, joined in zip(earlier, later, merged)
        )
    )


def expert_terms(arrived, gate_weight, up_weight, down_weight):
    local_experts = gate_weight.shape[0]
    sources = arrived.shape[0] // local_experts
    grouped = arrived.reshape(sources, local_experts, arrived.shape[1], arrived.shape[2])
    gate = jnp.einsum("secd,edf->secf", grouped, gate_weight, preferred_element_type=jnp.float32)
    upper = jnp.einsum("secd,edf->secf", grouped, up_weight, preferred_element_type=jnp.float32)
    hidden = (jax.nn.silu(gate) * upper).astype(jnp.bfloat16)
    output = jnp.einsum("secf,efd->secd", hidden, down_weight, preferred_element_type=jnp.float32)
    return output.reshape(arrived.shape[0], arrived.shape[1], down_weight.shape[2])


def plain_body(
    pool_input,
    doc_ids,
    residual,
    pool_gain,
    out_proj,
    norm_gain,
    routes,
    route_weights,
    expert_gate,
    expert_up,
    expert_down,
    shared_gate,
    shared_up,
    shared_down,
):
    row_count, channels = pool_input.shape
    values = pool_input.astype(jnp.float32)
    positions = jnp.arange(row_count, dtype=jnp.int32)
    inner_begin = jnp.concatenate([jnp.zeros((1,), bool), doc_ids[1:] != doc_ids[:-1]])
    running = jnp.cumsum(values[:, 3::4], axis=0)
    shifted = jnp.concatenate([jnp.zeros((1, running.shape[1]), jnp.float32), running], 0)
    inner_last = jnp.max(jnp.where(inner_begin, positions, 0))
    own_terms = (
        running[-1] - shifted[inner_last],
        (row_count - inner_last).astype(jnp.float32),
        doc_ids[0].astype(jnp.float32),
        doc_ids[-1].astype(jnp.float32),
        jnp.any(inner_begin).astype(jnp.float32),
    )
    identity = (
        jnp.zeros((running.shape[1],), jnp.float32),
        jnp.zeros((), jnp.float32),
        jnp.full((), -1.0, jnp.float32),
        jnp.full((), -1.0, jnp.float32),
        jnp.zeros((), jnp.float32),
    )
    before = carried_in(own_terms, "sp", join_documents, identity)
    fresh = (before[2] < 0) | (doc_ids[0].astype(jnp.float32) != before[3])
    begins = jnp.concatenate([fresh[None], inner_begin[1:]])
    doc_start = lax.cummax(jnp.where(begins, positions, -1), axis=0)
    found = doc_start >= 0
    carry_sum = jnp.where(fresh, 0.0, before[0])
    carry_length = jnp.where(fresh, 0.0, before[1])
    length = jnp.where(
        found,
        (positions - doc_start + 1).astype(jnp.float32),
        carry_length + (positions + 1).astype(jnp.float32),
    )
    start_rows = jnp.take(shifted, jnp.maximum(doc_start, 0), axis=0)
    doc_sum = jnp.where(found[:, None], running - start_rows, carry_sum[None, :] + running)
    doc_mean = doc_sum / length[:, None]
    rim = from_behind(pool_input[row_count - 15 :], "sp", 1)
    extended = jnp.concatenate([rim, pool_input], 0).astype(jnp.float32)
    scale_index = jnp.arange(channels, dtype=jnp.int32) % 4
    window_size = jnp.where(scale_index == 0, 2.0, jnp.where(scale_index == 1, 8.0, 16.0))
    window_total = jnp.zeros((row_count, channels), jnp.float32)
    for offset in range(16):
        inside = (offset < length[:, None]) & (offset < window_size[None, :])
        window_total = window_total + jnp.where(
            inside, extended[15 - offset : 15 - offset + row_count], 0.0
        )
    window_mean = window_total / jnp.minimum(length[:, None], window_size[None, :])
    pool_mean = jnp.concatenate(
        [window_mean.reshape(row_count, channels // 4, 4)[..., :3], doc_mean[..., None]], -1
    )
    pool_mean = pool_mean.reshape(row_count, channels)
    pooled = ((pool_mean - values) * pool_gain).astype(jnp.bfloat16)
    terms = jnp.dot(pooled, out_proj, preferred_element_type=jnp.float32)
    projected = lax.psum_scatter(terms.astype(jnp.bfloat16), "tp", scatter_dimension=1, tiled=True)
    hidden_state = residual.astype(jnp.float32) + projected.astype(jnp.float32)
    squares = lax.psum(jnp.sum(hidden_state * hidden_state, axis=1), "tp")
    model_width = residual.shape[1] * lax.axis_size("tp")
    scaling = lax.rsqrt(squares / model_width + 1e-06)
    normed_columns = (hidden_state * scaling[:, None] * norm_gain).astype(jnp.bfloat16)
    normed = lax.all_gather(normed_columns, "tp", axis=1, tiled=True)
    shared_gate_out = jnp.dot(normed, shared_gate, preferred_element_type=jnp.float32)
    shared_up_out = jnp.dot(normed, shared_up, preferred_element_type=jnp.float32)
    shared_hidden = (jax.nn.silu(shared_gate_out) * shared_up_out).astype(jnp.bfloat16)
    shared_terms = jnp.dot(shared_hidden, shared_down, preferred_element_type=jnp.float32)
    group_size = lax.axis_size("tp")
    experts = expert_gate.shape[0] * lax.axis_size("sp")
    top = routes.shape[1]
    capacity = group_size * max(1, 2 * row_count * top // (experts * group_size))
    flat_experts = routes.reshape(-1)
    onehot = (flat_experts[:, None] == jnp.arange(experts, dtype=jnp.int32)[None, :]).astype(
        jnp.int32
    )
    ranks = jnp.sum((jnp.cumsum(onehot, axis=0) - 1) * onehot, axis=1)
    slots = flat_experts * capacity + ranks
    token_index = jnp.arange(row_count * top, dtype=jnp.int32) // top
    slot_token = jnp.full((experts * capacity,), row_count, jnp.int32).at[slots].set(token_index)
    with_blank = jnp.concatenate([normed, jnp.zeros((1, normed.shape[1]), jnp.bfloat16)], 0)
    outgoing = jnp.take(with_blank, slot_token, axis=0).reshape(experts, capacity, normed.shape[1])
    share = capacity // group_size
    mine = lax.dynamic_slice_in_dim(outgoing, lax.axis_index("tp") * share, share, 1)
    arrived = lax.all_to_all(mine, "sp", split_axis=0, concat_axis=0, tiled=True)
    run_arrived = lax.all_gather(arrived, "tp", axis=1, tiled=True)
    expert_parts = expert_terms(run_arrived, expert_gate, expert_up, expert_down)
    routed_sum, shared_sum = (
        lax.psum_scatter(
            expert_parts.astype(jnp.bfloat16), "tp", scatter_dimension=2, tiled=True
        ).astype(jnp.float32),
        lax.psum_scatter(
            shared_terms[None].astype(jnp.bfloat16), "tp", scatter_dimension=2, tiled=True
        ).astype(jnp.float32),
    )
    returned = lax.all_to_all(
        routed_sum.astype(jnp.bfloat16), "sp", split_axis=0, concat_axis=0, tiled=True
    )
    flat_back = returned.reshape(experts * capacity, returned.shape[2])
    picked = (
        jnp.take(flat_back, slots, axis=0).astype(jnp.float32) * route_weights.reshape(-1)[:, None]
    )
    routed = jnp.sum(picked.reshape(row_count, top, flat_back.shape[1]), axis=1)
    shared_out = shared_sum[0].astype(jnp.bfloat16).astype(jnp.float32)
    return (hidden_state + routed + shared_out).astype(jnp.bfloat16)


F32 = jnp.float32
BF16 = jnp.bfloat16


def dot(a, b):
    return jnp.dot(a, b, preferred_element_type=F32)


def silu(v):
    return v * jax.nn.sigmoid(v)


def layer_kernel(
    groups,
    pool_ref, doc_ref, routes_ref, weights_ref, resid_ref, gain_ref, ngain_ref,
    oproj_hbm, eg_hbm, eu_hbm, ed_hbm, sg_hbm, su_hbm, sd_hbm,
    out_ref,
    oproj, eg, eu, ed, sg, su, sd, wsem,
    stat_out, stat_in, halo_in, stat_ss, stat_rs, halo_sem,
    s1, p1, q1, z1, r1_ss, r1_rs,
    ss_out, ss_in, ss_ss, ss_rs,
    sel, both, sc_out, sc_in, sc_ss, sc_rs, disp, rows, d_ss, d_rs, ag_ss, ag_rs,
    normed_ref, xs, xs_ss, xs_rs,
    s3, p3, q3, z3, r3_ss, r3_rs,
    hid, s2, p2, q2, z2, r2_ss, r2_rs,
    back, ret, b_ss, b_rs,
    hidden_ref,
):
    n = lax.axis_size("sp")
    tps = lax.axis_size("tp")
    me = lax.axis_index("sp")
    mt = lax.axis_index("tp")
    core = lax.rem(mt, 2)
    yy = mt // 2
    mate = yy * 2 + (1 - core)
    across = (1 - yy) * 2 + core
    R, C = pool_ref.shape
    DT = resid_ref.shape[1]
    D = DT * tps
    cap = disp.shape[1]

    loads = []
    for i, (src, dst) in enumerate(
        ((oproj_hbm, oproj), (sg_hbm, sg), (su_hbm, su), (sd_hbm, sd),
         (eg_hbm.at[0], eg), (eu_hbm.at[0], eu), (ed_hbm.at[0], ed))
    ):
        load = pltpu.make_async_copy(src, dst, wsem.at[i])
        load.start()
        loads.append(load)

    def peer(k):
        return me ^ k

    barrier = pltpu.get_barrier_semaphore()
    for k in range(1, n):
        pl.semaphore_signal(barrier, inc=1, device_id={"sp": peer(k)},
                            device_id_type=pl.DeviceIdType.MESH)
    for j in range(1, tps):
        pl.semaphore_signal(barrier, inc=1, device_id={"tp": lax.rem(mt + j, tps)},
                            device_id_type=pl.DeviceIdType.MESH)

    sends = []

    def send(src, dst, ss, rs, where):
        copy = pltpu.make_async_remote_copy(
            src_ref=src, dst_ref=dst, send_sem=ss, recv_sem=rs,
            device_id=where, device_id_type=pl.DeviceIdType.MESH)
        copy.start()
        sends.append(copy)

    def arrived(ref, ss, rs, where):
        pltpu.make_async_remote_copy(
            src_ref=ref, dst_ref=ref, send_sem=ss, recv_sem=rs,
            device_id=where, device_id_type=pl.DeviceIdType.MESH).wait_recv()

    doc = doc_ref[...].astype(F32)
    first = jnp.min(doc, axis=1, keepdims=True)
    last = jnp.max(doc, axis=1, keepdims=True)
    pool = pool_ref[...]
    tail_mask = jnp.broadcast_to((doc == last).astype(F32), (8, R))
    stat_out[...] = jnp.zeros_like(stat_out)
    stat_out[0:1, :] = dot(tail_mask.astype(BF16), pool)[0:1]
    stat_out[1:2, :] = jnp.broadcast_to(last, (1, C))
    stat_out[2:3, :] = jnp.broadcast_to(jnp.sum(tail_mask[0:1], axis=1, keepdims=True), (1, C))
    stat_out[3:4, 0:R] = pltpu.roll(jnp.broadcast_to(doc, (8, R)), 16, axis=1)[0:1]

    t_pos = lax.broadcasted_iota(jnp.int32, (R, R), 0)
    u_pos = lax.broadcasted_iota(jnp.int32, (R, R), 1)
    gap = t_pos - u_pos
    doc_row = jnp.broadcast_to(doc, (R, R))
    doc_col = doc_row.T

    pl.semaphore_wait(barrier, n - 1 + tps - 1)
    following = jnp.minimum(me + 1, n - 1)

    @pl.when(me < n - 1)
    def _():
        pltpu.make_async_remote_copy(
            src_ref=pool_ref.at[pl.ds(R - 16, 16)], dst_ref=halo_in,
            send_sem=halo_sem.at[0], recv_sem=halo_sem.at[1],
            device_id={"sp": following}, device_id_type=pl.DeviceIdType.MESH).start()

    for k in range(1, n):
        send(stat_out, stat_in.at[k], stat_ss.at[k], stat_rs.at[k], {"sp": peer(k)})

    same = (doc_col == doc_row) & (gap >= 0)
    length = jnp.sum(same.astype(F32), axis=1, keepdims=True)
    windows = (2, 8, 16)
    totals = [dot((same & (gap < w)).astype(F32).astype(BF16), pool) for w in windows]
    totals.append(dot(same.astype(F32).astype(BF16), pool))

    e_iota = lax.broadcasted_iota(jnp.int32, (n, R), 0)
    picked = (e_iota ^ me).astype(F32)
    routes = routes_ref[...].astype(F32)
    r0 = (jnp.broadcast_to(routes[0:1], (n, R)) == picked).astype(F32)
    r1 = (jnp.broadcast_to(routes[1:2], (n, R)) == picked).astype(F32)
    member = r0 + r1
    rank = dot(member.astype(BF16), (gap < 0).astype(F32).astype(BF16))
    slot = lax.broadcasted_iota(jnp.int32, (cap, R), 0).astype(F32)
    for p in range(n):
        here = (jnp.broadcast_to(rank[p:p + 1], (cap, R)) == slot).astype(F32)
        sel[0, p * cap:(p + 1) * cap, :] = (here * r0[p:p + 1]).astype(BF16)
        sel[1, p * cap:(p + 1) * cap, :] = (here * r1[p:p + 1]).astype(BF16)
        both[p * cap:(p + 1) * cap, :] = (here * member[p:p + 1]).astype(BF16)

    @pl.when(me > 0)
    def _():
        arrived(halo_in, halo_sem.at[0], halo_sem.at[1], {"sp": peer(1)})

    for k in range(1, n):
        arrived(stat_in.at[k], stat_ss.at[k], stat_rs.at[k], {"sp": peer(k)})
    carry = jnp.zeros((1, C), F32)
    carry_length = jnp.zeros((1, 1), F32)
    before_doc = jnp.zeros((1, R), F32)
    for k in range(1, n):
        source = jnp.full((1, C), peer(k), jnp.int32)
        use = (stat_in[k, 1:2, :] == jnp.broadcast_to(first, (1, C))) & (source < me)
        carry = carry + jnp.where(use, stat_in[k, 0:1, :], 0.0)
        carry_length = carry_length + jnp.where(use, stat_in[k, 2:3, :], 0.0)[:, 0:1]
        before_doc = before_doc + jnp.where(source[:, 0:R] == me - 1, stat_in[k, 3:4, 0:R], 0.0)
    in_first = (doc_col == first).astype(F32)[:, 0:1]
    length = length + in_first * carry_length
    halo_doc = jnp.broadcast_to(before_doc, (R, R))
    reach = gap + 16
    halo_ok = (halo_doc == doc_col) & (jnp.full((R, R), me, jnp.int32) > 0)
    halo = jnp.where(jnp.full(halo_in.shape, me, jnp.int32) > 0, halo_in[...].astype(F32), 0.0).astype(BF16)
    totals = [
        total + dot((halo_ok & (reach < w)).astype(F32)[:, 0:16].astype(BF16), halo)
        for total, w in zip(totals, windows)
    ] + [totals[3] + in_first * carry]
    lane = lax.rem(lax.broadcasted_iota(jnp.int32, (R, C), 1), 4)
    mean = totals[3] / length
    for i, w in enumerate(windows):
        mean = jnp.where(lane == i, totals[i] / jnp.minimum(length, float(w)), mean)
    pooled = ((mean - pool.astype(F32)) * gain_ref[...]).astype(BF16)

    def scatter_start(s, p, ss, rs):
        for i, y2 in enumerate((1 - yy, yy)):
            send(s.at[y2 * 2 + 1 - core], p.at[i], ss.at[i], rs.at[i], {"tp": mate})

    def scatter_across(s, p, q, z, ss, rs):
        arrived(p.at[0], ss.at[0], rs.at[0], {"tp": mate})
        q[...] = (s[across].astype(F32) + p[0].astype(F32)).astype(BF16)
        send(q, z, ss.at[2], rs.at[2], {"tp": across})

    def scatter_end(s, p, z, ss, rs):
        arrived(p.at[1], ss.at[1], rs.at[1], {"tp": mate})
        own = s[mt].astype(F32) + p[1].astype(F32)
        arrived(z, ss.at[2], rs.at[2], {"tp": across})
        return own + z[...].astype(F32)

    loads[0].wait()
    for j in range(tps):
        s1[j] = dot(pooled, oproj[:, j * DT:(j + 1) * DT]).astype(BF16)
    scatter_start(s1, p1, r1_ss, r1_rs)
    scatter_across(s1, p1, q1, z1, r1_ss, r1_rs)
    projected = scatter_end(s1, p1, z1, r1_ss, r1_rs)
    hidden = resid_ref[...].astype(F32) + projected
    hidden_ref[...] = hidden
    squares = jnp.sum(hidden * hidden, axis=1, keepdims=True)
    sq_row = jnp.broadcast_to(squares, (R, R)).T
    ss_out[...] = sq_row[0:8]
    for j in range(1, tps):
        send(ss_out, ss_in.at[j], ss_ss.at[j], ss_rs.at[j], {"tp": lax.rem(mt + j, tps)})
    normed = (hidden * ngain_ref[...]).astype(BF16)
    normed_ref[...] = normed

    for p in range(1, n):
        disp[p] = dot(both[p * cap:(p + 1) * cap, :], normed).astype(BF16)
        send(disp.at[p], rows.at[p, mt], d_ss.at[p], d_rs.at[p], {"sp": peer(p)})

    send(normed_ref, xs.at[mt], xs_ss.at[0], xs_rs.at[0], {"tp": across})
    send(normed_ref, xs.at[mt], xs_ss.at[1], xs_rs.at[1], {"tp": mate})
    xs[mt] = normed

    all_sq = sq_row[0:8]
    for j in range(1, tps):
        arrived(ss_in.at[j], ss_ss.at[j], ss_rs.at[j], {"tp": mt})
        all_sq = all_sq + ss_in[j]
    scale_row = lax.rsqrt(all_sq / D + 1e-06)
    high = scale_row.astype(BF16)
    rest = scale_row - high.astype(F32)
    middle = rest.astype(BF16)
    low = (rest - middle.astype(F32)).astype(BF16)
    turned = (((1,), (1,)), ((), ()))
    slot_scale = sum(
        lax.dot_general(part, both[...], turned, preferred_element_type=F32) for part in (high, middle, low))
    for p in range(n):
        sc_out[p, :, 0:cap] = slot_scale[:, p * cap:(p + 1) * cap]
        if p:
            send(sc_out.at[p], sc_in.at[p], sc_ss.at[p], sc_rs.at[p], {"sp": peer(p)})
    scale = jnp.broadcast_to(scale_row[0:1], (R, R)).T[:, 0:1]

    def forward_own(ps):
        for p in ps:
            arrived(rows.at[p, mt], d_ss.at[p], d_rs.at[p], {"sp": peer(p)})
            send(rows.at[p, mt], rows.at[p, mt], ag_ss.at[p, 0], ag_rs.at[p, 0], {"tp": across})
            send(rows.at[p, mt], rows.at[p, mt], ag_ss.at[p, 1], ag_rs.at[p, 1], {"tp": mate})

    def forward_across(ps):
        for p in ps:
            arrived(rows.at[p, across], ag_ss.at[p, 0], ag_rs.at[p, 0], {"tp": across})
            send(rows.at[p, across], rows.at[p, across], ag_ss.at[p, 2], ag_rs.at[p, 2], {"tp": mate})

    def all_here(ps):
        for p in ps:
            if p:
                arrived(rows.at[p, mate], ag_ss.at[p, 1], ag_rs.at[p, 1], {"tp": mate})
                arrived(rows.at[p, (1 - yy) * 2 + 1 - core], ag_ss.at[p, 2], ag_rs.at[p, 2], {"tp": mate})
                arrived(sc_in.at[p], sc_ss.at[p], sc_rs.at[p], {"sp": peer(p)})

    def shared():
        for load in loads[1:4]:
            load.wait()
        g = sum(dot(xs[j], sg[j * DT:(j + 1) * DT, :]) for j in range(tps)) * scale
        u = sum(dot(xs[j], su[j * DT:(j + 1) * DT, :]) for j in range(tps)) * scale
        hs = (silu(g) * u).astype(BF16)
        for j in range(tps):
            s3[j] = dot(hs, sd[:, j * DT:(j + 1) * DT]).astype(BF16)
        scatter_start(s3, p3, r3_ss, r3_rs)

    FF = eg.shape[1]
    tile = 256 if FF % 256 == 0 else FF

    def expert_up(gi):
        ps = groups[gi]
        m = len(ps) * cap
        factors = []
        for p in ps:
            line = (sc_in if p else sc_out)[p, 0:1, :]
            factors.append(jnp.broadcast_to(line, (128, 128)).T[0:cap, 0:1])
        factor = jnp.concatenate(factors, 0)

        def up(i, _):
            cols = pl.ds(pl.multiple_of(i * tile, tile), tile)
            a = jnp.zeros((m, tile), F32)
            b = jnp.zeros((m, tile), F32)
            for j in range(tps):
                x = rows[ps[0]:ps[0] + len(ps), j].reshape(m, DT)
                a = a + dot(x, eg[j * DT:(j + 1) * DT, cols])
                b = b + dot(x, eu[j * DT:(j + 1) * DT, cols])
            hid[0:m, cols] = (silu(a * factor) * (b * factor)).astype(BF16)
            return 0

        lax.fori_loop(0, FF // tile, up, 0)

    def expert_down(gi):
        m = len(groups[gi]) * cap
        s, p, _, _, ss, rs = scatter_refs(gi)

        def down(j):
            s[j] = dot(hid[0:m, :], ed[:, pl.ds(pl.multiple_of(j * DT, DT), DT)]).astype(BF16)

        for i, y2 in enumerate((1 - yy, yy)):
            down(y2 * 2 + 1 - core)
            send(s.at[y2 * 2 + 1 - core], p.at[i], ss.at[i], rs.at[i], {"tp": mate})
            down(y2 * 2 + core)

    def scatter_refs(gi):
        span = pl.ds(groups[gi][0] * cap, len(groups[gi]) * cap)
        return (s2.at[:, span], p2.at[:, span], q2.at[span], z2.at[span], r2_ss.at[gi], r2_rs.at[gi])

    def across2(gi):
        scatter_across(*scatter_refs(gi))

    def give_back(gi):
        s, p, q, z, ss, rs = scatter_refs(gi)
        total = scatter_end(s, p, z, ss, rs).astype(BF16)
        for i, p in enumerate(groups[gi]):
            piece = total[i * cap:(i + 1) * cap]
            if p == 0:
                ret[0:cap, :] = piece
            else:
                back[p] = piece
                send(back.at[p], ret.at[pl.ds(p * cap, cap)], b_ss.at[p], b_rs.at[p], {"sp": peer(p)})

    def collect(gi):
        span = pl.ds(groups[gi][0] * cap, len(groups[gi]) * cap)
        for p in groups[gi]:
            if p:
                arrived(ret.at[pl.ds(p * cap, cap)], b_ss.at[p], b_rs.at[p], {"sp": peer(p)})
        total = hidden_ref[...]
        for k in range(2):
            weight = jnp.broadcast_to(weights_ref[k:k + 1, :], (R, R)).T[:, 0:1]
            chosen = lax.dot_general(
                sel[k, span], ret[span], (((0,), (0,)), ((), ())), preferred_element_type=F32)
            total = total + weight * chosen
        return total

    near, far, last_far = 0, 1, 2
    forward_own(groups[near][1:])
    arrived(xs.at[across], xs_ss.at[0], xs_rs.at[0], {"tp": across})
    send(xs.at[across], xs.at[across], xs_ss.at[2], xs_rs.at[2], {"tp": mate})
    arrived(xs.at[mate], xs_ss.at[1], xs_rs.at[1], {"tp": mate})
    arrived(xs.at[(1 - yy) * 2 + 1 - core], xs_ss.at[2], xs_rs.at[2], {"tp": mate})
    for j in range(tps):
        rows[0, j] = dot(both[0:cap, :], xs[j]).astype(BF16)
    forward_across(groups[near][1:])
    for load in loads[4:]:
        load.wait()
    all_here(groups[near])
    expert_up(near)
    forward_own(groups[far])
    expert_down(near)
    forward_own(groups[last_far])
    shared()
    across2(near)
    forward_across(groups[far])
    all_here(groups[far])
    expert_up(far)
    forward_across(groups[last_far])
    scatter_across(s3, p3, q3, z3, r3_ss, r3_rs)
    expert_down(far)
    give_back(near)
    across2(far)
    all_here(groups[last_far])
    expert_up(last_far)
    expert_down(last_far)
    give_back(far)
    across2(last_far)
    hidden_ref[...] = hidden_ref[...] + scatter_end(s3, p3, z3, r3_ss, r3_rs).astype(BF16).astype(F32)
    hidden_ref[...] = collect(near)
    give_back(last_far)
    hidden_ref[...] = collect(far)
    result = collect(last_far)
    out_ref[...] = result.astype(BF16)
    for copy in sends:
        copy.wait_send()

    @pl.when(me < n - 1)
    def _():
        pltpu.make_async_remote_copy(
            src_ref=pool_ref.at[pl.ds(R - 16, 16)], dst_ref=halo_in,
            send_sem=halo_sem.at[0], recv_sem=halo_sem.at[1],
            device_id={"sp": following}, device_id_type=pl.DeviceIdType.MESH).wait_send()


def body(
    pool_input, doc_ids, residual, pool_gain, out_proj, norm_gain, routes, route_weights,
    expert_gate, expert_up, expert_down, shared_gate, shared_up, shared_down,
):
    n, tps = lax.axis_size("sp"), lax.axis_size("tp")
    R, C = pool_input.shape
    DT = residual.shape[1]
    FF, FS, D = expert_gate.shape[2], shared_gate.shape[1], expert_gate.shape[1]
    experts = expert_gate.shape[0] * n
    top = routes.shape[1]
    cap = tps * max(1, 2 * R * top // (experts * tps))
    groups = [list(range(n // 2)), list(range(n // 2, 3 * n // 4)), list(range(3 * n // 4, n))]
    m = cap * n // 2
    V, DMA = pltpu.VMEM, pltpu.SemaphoreType.DMA
    scratch = [
        V((C, D), BF16), V((D, FF), BF16), V((D, FF), BF16), V((FF, D), BF16),
        V((D, FS), BF16), V((D, FS), BF16), V((FS, D), BF16), DMA((7,)),
        V((8, C), F32), V((n, 8, C), F32), V((16, C), BF16), DMA((n,)), DMA((n,)), DMA((2,)),
        V((tps, R, DT), BF16), V((2, R, DT), BF16), V((R, DT), BF16), V((R, DT), BF16), DMA((3,)), DMA((3,)),
        V((8, R), F32), V((tps, 8, R), F32), DMA((tps,)), DMA((tps,)),
        V((2, n * cap, R), BF16), V((n * cap, R), BF16), V((n, 8, 128), F32), V((n, 8, 128), F32), DMA((n,)), DMA((n,)),
        V((n, cap, DT), BF16), V((n, tps, cap, DT), BF16),
        DMA((n,)), DMA((n,)), DMA((n, 3)), DMA((n, 3)),
        V((R, DT), BF16), V((tps, R, DT), BF16), DMA((3,)), DMA((3,)),
        V((tps, R, DT), BF16), V((2, R, DT), BF16), V((R, DT), BF16), V((R, DT), BF16), DMA((3,)), DMA((3,)),
        V((m, FF), BF16), V((tps, n * cap, DT), BF16), V((2, n * cap, DT), BF16),
        V((n * cap, DT), BF16), V((n * cap, DT), BF16), DMA((3, 3)), DMA((3, 3)),
        V((n, cap, DT), BF16), V((n * cap, DT), BF16), DMA((n,)), DMA((n,)),
        V((R, DT), F32),
    ]
    vm = pl.BlockSpec(memory_space=pltpu.VMEM)
    hb = pl.BlockSpec(memory_space=pl.ANY)
    return pl.pallas_call(
        functools.partial(layer_kernel, groups),
        out_shape=jax.ShapeDtypeStruct((R, DT), BF16),
        in_specs=[vm] * 7 + [hb] * 7,
        out_specs=vm,
        scratch_shapes=scratch,
        compiler_params=pltpu.CompilerParams(
            collective_id=0, has_side_effects=True, vmem_limit_bytes=60 * 2**20),
    )(pool_input, doc_ids.reshape(1, R), routes.T, route_weights.T, residual, pool_gain.reshape(1, C), norm_gain.reshape(1, DT),
      out_proj, expert_gate, expert_up, expert_down, shared_gate, shared_up, shared_down)


def one_kernel_fits(mesh):
    return mesh.shape["tp"] == 4 and mesh.shape["sp"] == 8


def solution(mesh):
    placed = (
        P("sp", "tp"),
        P("sp"),
        P("sp", "tp"),
        P("tp"),
        P("tp", None),
        P("tp"),
        P("sp", None),
        P("sp", None),
        P("sp", None, "tp"),
        P("sp", None, "tp"),
        P("sp", "tp", None),
        P(None, "tp"),
        P(None, "tp"),
        P("tp", None),
    )
    return jax.shard_map(
        body if one_kernel_fits(mesh) else plain_body, mesh=mesh, in_specs=placed, out_specs=P("sp", "tp"), check_vma=False)
```

profile of v0, /device:TPU:0, one launch (start us, length us, event | category | flops | bytes accessed | tf_op | source)
XLA Modules:
  0.0 65.8 jit_solution(6749760363861119322)
XLA Ops:
  0.0 64.2 %shard_map.136 = bf16[128,512]{1,0:T(8,128)(2,1)} custom-call(bf16[128,256]{1,0:T(8,128)(2,1)} %pool_ref.1, s32[1,128]{1,0:T(1,128)} %bitcast.9, s32[2,128]{1,0:T(2,128)} %bitcast.6, f32[2,128]{1,0:T(2,128)} %bitcast.7, bf16[128,512]{1,0:T(8,128)(2,1)} %resid_ref.1, f32[1,256]{1,0:T(1,128)} %bitcast.8, f32[1,512]{1,0:T(1,128)} %bitcast.5, ...), custom_call_target="tpu_custom_call" | custom-call | tf_op jit(solution)/shard_map/pallas_call | solution.py:571
  64.3 1.6 %copy.16 = bf16[128,512]{1,0:T(8,128)(2,1)} copy(bf16[128,512]{1,0:T(8,128)(2,1)} %shard_map.136) | data formatting | bytes 262144
where the time goes:
time: 66 us; the launch traced here: 65.8 us
  Pallas kernels  64.2 us (97%)
  local copies, waits for them, and re-layouts  1.57 us (2%)
    pallas_call x1, Pallas kernels, body(): pl.pallas_call(functools.partial(layer_kernel, groups), out_shape=jax.Sha...  64.2 us
    unnamed x1, local copies, waits for them, and re-layouts  1.57 us

commit v1 on v0

--- a/solution.py
+++ b/solution.py
@@ -193,9 +193,9 @@
 
 def layer_kernel(
     groups,
-    pool_ref, doc_ref, routes_ref, weights_ref, resid_ref, gain_ref, ngain_ref,
-    oproj_hbm, eg_hbm, eu_hbm, ed_hbm, sg_hbm, su_hbm, sd_hbm,
+    pool_hbm, doc_hbm, routes_hbm, weights_hbm, resid_hbm, gain_hbm, ngain_hbm, oproj_hbm, eg_hbm, eu_hbm, ed_hbm, sg_hbm, su_hbm, sd_hbm,
     out_ref,
+    pool_ref, doc_ref, routes_ref, weights_ref, resid_ref, gain_ref, ngain_ref, isem,
     oproj, eg, eu, ed, sg, su, sd, wsem,
     stat_out, stat_in, halo_in, stat_ss, stat_rs, halo_sem,
     s1, p1, q1, z1, r1_ss, r1_rs,
@@ -220,15 +220,6 @@
     D = DT * tps
     cap = disp.shape[1]
 
-    loads = []
-    for i, (src, dst) in enumerate(
-        ((oproj_hbm, oproj), (sg_hbm, sg), (su_hbm, su), (sd_hbm, sd),
-         (eg_hbm.at[0], eg), (eu_hbm.at[0], eu), (ed_hbm.at[0], ed))
-    ):
-        load = pltpu.make_async_copy(src, dst, wsem.at[i])
-        load.start()
-        loads.append(load)
-
     def peer(k):
         return me ^ k
 
@@ -240,6 +231,20 @@
         pl.semaphore_signal(barrier, inc=1, device_id={"tp": lax.rem(mt + j, tps)},
                             device_id_type=pl.DeviceIdType.MESH)
 
+    small = [
+        pltpu.make_async_copy(src, dst, isem.at[i])
+        for i, (src, dst) in enumerate((
+            (doc_hbm, doc_ref), (pool_hbm, pool_ref), (routes_hbm, routes_ref), (gain_hbm, gain_ref),
+            (resid_hbm, resid_ref), (ngain_hbm, ngain_ref), (weights_hbm, weights_ref)))
+    ]
+    loads = [
+        pltpu.make_async_copy(src, dst, wsem.at[i])
+        for i, (src, dst) in enumerate((
+            (oproj_hbm, oproj), (sg_hbm, sg), (su_hbm, su), (sd_hbm, sd),
+            (eg_hbm.at[0], eg), (eu_hbm.at[0], eu), (ed_hbm.at[0], ed)))
+    ]
+    for load in small + loads:
+        load.start()
     sends = []
 
     def send(src, dst, ss, rs, where):
@@ -254,6 +259,8 @@
             src_ref=ref, dst_ref=ref, send_sem=ss, recv_sem=rs,
             device_id=where, device_id_type=pl.DeviceIdType.MESH).wait_recv()
 
+    small[0].wait()
+    small[1].wait()
     doc = doc_ref[...].astype(F32)
     first = jnp.min(doc, axis=1, keepdims=True)
     last = jnp.max(doc, axis=1, keepdims=True)
@@ -292,6 +299,7 @@
 
     e_iota = lax.broadcasted_iota(jnp.int32, (n, R), 0)
     picked = (e_iota ^ me).astype(F32)
+    small[2].wait()
     routes = routes_ref[...].astype(F32)
     r0 = (jnp.broadcast_to(routes[0:1], (n, R)) == picked).astype(F32)
     r1 = (jnp.broadcast_to(routes[1:2], (n, R)) == picked).astype(F32)
@@ -333,6 +341,7 @@
     mean = totals[3] / length
     for i, w in enumerate(windows):
         mean = jnp.where(lane == i, totals[i] / jnp.minimum(length, float(w)), mean)
+    small[3].wait()
     pooled = ((mean - pool.astype(F32)) * gain_ref[...]).astype(BF16)
 
     def scatter_start(s, p, ss, rs):
@@ -356,6 +365,8 @@
     scatter_start(s1, p1, r1_ss, r1_rs)
     scatter_across(s1, p1, q1, z1, r1_ss, r1_rs)
     projected = scatter_end(s1, p1, z1, r1_ss, r1_rs)
+    for load in small[4:]:
+        load.wait()
     hidden = resid_ref[...].astype(F32) + projected
     hidden_ref[...] = hidden
     squares = jnp.sum(hidden * hidden, axis=1, keepdims=True)
@@ -366,12 +377,13 @@
     normed = (hidden * ngain_ref[...]).astype(BF16)
     normed_ref[...] = normed
 
-    for p in range(1, n):
-        disp[p] = dot(both[p * cap:(p + 1) * cap, :], normed).astype(BF16)
-        send(disp.at[p], rows.at[p, mt], d_ss.at[p], d_rs.at[p], {"sp": peer(p)})
-
     send(normed_ref, xs.at[mt], xs_ss.at[0], xs_rs.at[0], {"tp": across})
     send(normed_ref, xs.at[mt], xs_ss.at[1], xs_rs.at[1], {"tp": mate})
+    for ps in (list(range(1, n // 2)), list(range(n // 2, n))):
+        span = slice(ps[0] * cap, (ps[-1] + 1) * cap)
+        disp[ps[0]:ps[-1] + 1] = dot(both[span, :], normed).astype(BF16).reshape(len(ps), cap, DT)
+        for p in ps:
+            send(disp.at[p], rows.at[p, mt], d_ss.at[p], d_rs.at[p], {"sp": peer(p)})
     xs[mt] = normed
 
     all_sq = sq_row[0:8]
@@ -392,23 +404,45 @@
             send(sc_out.at[p], sc_in.at[p], sc_ss.at[p], sc_rs.at[p], {"sp": peer(p)})
     scale = jnp.broadcast_to(scale_row[0:1], (R, R)).T[:, 0:1]
 
-    def forward_own(ps):
+    def own_here(p):
+        arrived(rows.at[p, mt], d_ss.at[p], d_rs.at[p], {"sp": peer(p)})
+
+    def forward_own(*ps):
         for p in ps:
-            arrived(rows.at[p, mt], d_ss.at[p], d_rs.at[p], {"sp": peer(p)})
+            own_here(p)
             send(rows.at[p, mt], rows.at[p, mt], ag_ss.at[p, 0], ag_rs.at[p, 0], {"tp": across})
             send(rows.at[p, mt], rows.at[p, mt], ag_ss.at[p, 1], ag_rs.at[p, 1], {"tp": mate})
 
-    def forward_across(ps):
+    def forward_own2(*ps):
+        for p in ps:
+            send(rows.at[p, mt], rows.at[p, mt], ag_ss.at[p, 0], ag_rs.at[p, 0], {"tp": across})
+            send(rows.at[p, mt], rows.at[p, mt], ag_ss.at[p, 1], ag_rs.at[p, 1], {"tp": mate})
+
+    def forward_across(*ps):
         for p in ps:
             arrived(rows.at[p, across], ag_ss.at[p, 0], ag_rs.at[p, 0], {"tp": across})
             send(rows.at[p, across], rows.at[p, across], ag_ss.at[p, 2], ag_rs.at[p, 2], {"tp": mate})
 
-    def all_here(ps):
+    def all_here(*ps):
         for p in ps:
             if p:
                 arrived(rows.at[p, mate], ag_ss.at[p, 1], ag_rs.at[p, 1], {"tp": mate})
                 arrived(rows.at[p, (1 - yy) * 2 + 1 - core], ag_ss.at[p, 2], ag_rs.at[p, 2], {"tp": mate})
                 arrived(sc_in.at[p], sc_ss.at[p], sc_rs.at[p], {"sp": peer(p)})
+
+    def xs_across():
+        arrived(xs.at[across], xs_ss.at[0], xs_rs.at[0], {"tp": across})
+        send(xs.at[across], xs.at[across], xs_ss.at[2], xs_rs.at[2], {"tp": mate})
+
+    def xs_rest():
+        arrived(xs.at[mate], xs_ss.at[1], xs_rs.at[1], {"tp": mate})
+        arrived(xs.at[(1 - yy) * 2 + 1 - core], xs_ss.at[2], xs_rs.at[2], {"tp": mate})
+        for j in range(tps):
+            rows[0, j] = dot(both[0:cap, :], xs[j]).astype(BF16)
+
+    def weights_here():
+        for load in loads[4:]:
+            load.wait()
 
     def shared():
         for load in loads[1:4]:
@@ -420,10 +454,17 @@
             s3[j] = dot(hs, sd[:, j * DT:(j + 1) * DT]).astype(BF16)
         scatter_start(s3, p3, r3_ss, r3_rs)
 
+    def shared_across():
+        scatter_across(s3, p3, q3, z3, r3_ss, r3_rs)
+
+    def shared_end():
+        hidden_ref[...] = hidden_ref[...] + scatter_end(s3, p3, z3, r3_ss, r3_rs).astype(BF16).astype(F32)
+
     FF = eg.shape[1]
     tile = 256 if FF % 256 == 0 else FF
-
-    def expert_up(gi):
+    tiles = FF // tile
+
+    def expert_up(gi, start=0, stop=tiles):
         ps = groups[gi]
         m = len(ps) * cap
         factors = []
@@ -431,6 +472,7 @@
             line = (sc_in if p else sc_out)[p, 0:1, :]
             factors.append(jnp.broadcast_to(line, (128, 128)).T[0:cap, 0:1])
         factor = jnp.concatenate(factors, 0)
+        span = pl.ds(ps[0] * cap, m)
 
         def up(i, _):
             cols = pl.ds(pl.multiple_of(i * tile, tile), tile)
@@ -440,22 +482,23 @@
                 x = rows[ps[0]:ps[0] + len(ps), j].reshape(m, DT)
                 a = a + dot(x, eg[j * DT:(j + 1) * DT, cols])
                 b = b + dot(x, eu[j * DT:(j + 1) * DT, cols])
-            hid[0:m, cols] = (silu(a * factor) * (b * factor)).astype(BF16)
+            hid[span, cols] = (silu(a * factor) * (b * factor)).astype(BF16)
             return 0
 
-        lax.fori_loop(0, FF // tile, up, 0)
-
-    def expert_down(gi):
-        m = len(groups[gi]) * cap
+        lax.fori_loop(start, stop, up, 0)
+
+    def expert_down(gi, half):
+        span = pl.ds(groups[gi][0] * cap, len(groups[gi]) * cap)
         s, p, _, _, ss, rs = scatter_refs(gi)
 
         def down(j):
-            s[j] = dot(hid[0:m, :], ed[:, pl.ds(pl.multiple_of(j * DT, DT), DT)]).astype(BF16)
+            s[j] = dot(hid[span, :], ed[:, pl.ds(pl.multiple_of(j * DT, DT), DT)]).astype(BF16)
 
         for i, y2 in enumerate((1 - yy, yy)):
-            down(y2 * 2 + 1 - core)
-            send(s.at[y2 * 2 + 1 - core], p.at[i], ss.at[i], rs.at[i], {"tp": mate})
-            down(y2 * 2 + core)
+            if i in half:
+                down(y2 * 2 + 1 - core)
+                send(s.at[y2 * 2 + 1 - core], p.at[i], ss.at[i], rs.at[i], {"tp": mate})
+                down(y2 * 2 + core)
 
     def scatter_refs(gi):
         span = pl.ds(groups[gi][0] * cap, len(groups[gi]) * cap)
@@ -486,45 +529,56 @@
             chosen = lax.dot_general(
                 sel[k, span], ret[span], (((0,), (0,)), ((), ())), preferred_element_type=F32)
             total = total + weight * chosen
-        return total
-
-    near, far, last_far = 0, 1, 2
-    forward_own(groups[near][1:])
-    arrived(xs.at[across], xs_ss.at[0], xs_rs.at[0], {"tp": across})
-    send(xs.at[across], xs.at[across], xs_ss.at[2], xs_rs.at[2], {"tp": mate})
-    arrived(xs.at[mate], xs_ss.at[1], xs_rs.at[1], {"tp": mate})
-    arrived(xs.at[(1 - yy) * 2 + 1 - core], xs_ss.at[2], xs_rs.at[2], {"tp": mate})
-    for j in range(tps):
-        rows[0, j] = dot(both[0:cap, :], xs[j]).astype(BF16)
-    forward_across(groups[near][1:])
-    for load in loads[4:]:
-        load.wait()
-    all_here(groups[near])
-    expert_up(near)
-    forward_own(groups[far])
-    expert_down(near)
-    forward_own(groups[last_far])
+        hidden_ref[...] = total
+
+    forward_own(1)
+    xs_across()
+    forward_own(2)
+    forward_own(4)
+    forward_across(1)
+    xs_rest()
+    forward_own(5)
+    weights_here()
+    all_here(0, 1)
+    expert_up(0, 0, 2)
+    forward_own(3)
+    forward_across(2, 4)
+    expert_up(0, 2, 4)
+    forward_across(5)
+    forward_own(6)
+    expert_down(0, (0,))
+    forward_across(3)
+    expert_down(0, (1,))
+    forward_own(7)
+    all_here(4, 5)
+    expert_up(2, 0, 2)
+    forward_across(6)
+    across2(0)
+    expert_up(2, 2, 4)
+    expert_down(2, (0, 1))
+    forward_across(7)
     shared()
-    across2(near)
-    forward_across(groups[far])
-    all_here(groups[far])
-    expert_up(far)
-    forward_across(groups[last_far])
-    scatter_across(s3, p3, q3, z3, r3_ss, r3_rs)
-    expert_down(far)
-    give_back(near)
-    across2(far)
-    all_here(groups[last_far])
-    expert_up(last_far)
-    expert_down(last_far)
-    give_back(far)
-    across2(last_far)
-    hidden_ref[...] = hidden_ref[...] + scatter_end(s3, p3, z3, r3_ss, r3_rs).astype(BF16).astype(F32)
-    hidden_ref[...] = collect(near)
-    give_back(last_far)
-    hidden_ref[...] = collect(far)
-    result = collect(last_far)
-    out_ref[...] = result.astype(BF16)
+    across2(2)
+    all_here(6, 7)
+    expert_up(3)
+    give_back(0)
+    expert_down(3, (0, 1))
+    all_here(2, 3)
+    expert_up(1, 0, 2)
+    across2(3)
+    give_back(2)
+    expert_up(1, 2, 4)
+    expert_down(1, (0, 1))
+    collect(0)
+    give_back(3)
+    across2(1)
+    shared_across()
+    collect(2)
+    give_back(1)
+    shared_end()
+    collect(3)
+    collect(1)
+    out_ref[...] = hidden_ref[...].astype(BF16)
     for copy in sends:
         copy.wait_send()
 
@@ -547,10 +601,11 @@
     experts = expert_gate.shape[0] * n
     top = routes.shape[1]
     cap = tps * max(1, 2 * R * top // (experts * tps))
-    groups = [list(range(n // 2)), list(range(n // 2, 3 * n // 4)), list(range(3 * n // 4, n))]
-    m = cap * n // 2
+    groups = [[0, 1], [2, 3], [4, 5], [6, 7]]
     V, DMA = pltpu.VMEM, pltpu.SemaphoreType.DMA
     scratch = [
+        V((R, C), BF16), V((1, R), jnp.int32), V((top, R), jnp.int32), V((top, R), F32),
+        V((R, DT), BF16), V((1, C), F32), V((1, DT), F32), DMA((7,)),
         V((C, D), BF16), V((D, FF), BF16), V((D, FF), BF16), V((FF, D), BF16),
         V((D, FS), BF16), V((D, FS), BF16), V((FS, D), BF16), DMA((7,)),
         V((8, C), F32), V((n, 8, C), F32), V((16, C), BF16), DMA((n,)), DMA((n,)), DMA((2,)),
@@ -561,17 +616,17 @@
         DMA((n,)), DMA((n,)), DMA((n, 3)), DMA((n, 3)),
         V((R, DT), BF16), V((tps, R, DT), BF16), DMA((3,)), DMA((3,)),
         V((tps, R, DT), BF16), V((2, R, DT), BF16), V((R, DT), BF16), V((R, DT), BF16), DMA((3,)), DMA((3,)),
-        V((m, FF), BF16), V((tps, n * cap, DT), BF16), V((2, n * cap, DT), BF16),
-        V((n * cap, DT), BF16), V((n * cap, DT), BF16), DMA((3, 3)), DMA((3, 3)),
+        V((n * cap, FF), BF16), V((tps, n * cap, DT), BF16), V((2, n * cap, DT), BF16),
+        V((n * cap, DT), BF16), V((n * cap, DT), BF16), DMA((len(groups), 3)), DMA((len(groups), 3)),
         V((n, cap, DT), BF16), V((n * cap, DT), BF16), DMA((n,)), DMA((n,)),
         V((R, DT), F32),
     ]
     vm = pl.BlockSpec(memory_space=pltpu.VMEM)
-    hb = pl.BlockSpec(memory_space=pl.ANY)
+    hb = pl.BlockSpec(memory_space=pltpu.HBM)
     return pl.pallas_call(
         functools.partial(layer_kernel, groups),
         out_shape=jax.ShapeDtypeStruct((R, DT), BF16),
-        in_specs=[vm] * 7 + [hb] * 7,
+        in_specs=[hb] * 14,
         out_specs=vm,
         scratch_shapes=scratch,
         compiler_params=pltpu.CompilerParams(

time: 66 us -> 59.3 us (0.90)
  Pallas kernels: 64.2 us -> 57.5 us
    pallas_call x1, Pallas kernels: 64.2 us -> 57.5 us  [body(): pl.pallas_call(functools.partial(layer_kernel, groups), out_shape=jax.Sha...]
where the time goes in v1:
time: 59.3 us; the launch traced here: 59.1 us
  Pallas kernels  57.5 us (97%)
  local copies, waits for them, and re-layouts  1.57 us (3%)
    pallas_call x1, Pallas kernels, body(): pl.pallas_call(functools.partial(layer_kernel, groups), out_shape=jax.Sha...  57.5 us
    unnamed x1, local copies, waits for them, and re-layouts  1.57 us

profile of v1, /device:TPU:0, one launch (start us, length us, event | category | flops | bytes accessed | tf_op | source)
XLA Modules:
  0.0 59.1 jit_solution(8726921724752000374)
XLA Ops:
  0.0 57.5 %shard_map.136 = bf16[128,512]{1,0:T(8,128)(2,1)} custom-call(bf16[128,256]{1,0:T(8,128)(2,1)} %pool_hbm.1, s32[1,128]{1,0:T(1,128)} %bitcast.9, s32[2,128]{1,0:T(2,128)} %bitcast.6, f32[2,128]{1,0:T(2,128)} %bitcast.7, bf16[128,512]{1,0:T(8,128)(2,1)} %resid_hbm.1, f32[1,256]{1,0:T(1,128)} %bitcast.8, f32[1,512]{1,0:T(1,128)} %bitcast.5, ...), custom_call_target="tpu_custom_call" | custom-call | tf_op jit(solution)/shard_map/pallas_call | solution.py:626
  57.6 1.6 %copy.16 = bf16[128,512]{1,0:T(8,128)(2,1)} copy(bf16[128,512]{1,0:T(8,128)(2,1)} %shard_map.136) | data formatting | bytes 262144

commit v2 on v1

--- a/solution.py
+++ b/solution.py
@@ -203,7 +203,7 @@
     sel, both, sc_out, sc_in, sc_ss, sc_rs, disp, rows, d_ss, d_rs, ag_ss, ag_rs,
     normed_ref, xs, xs_ss, xs_rs,
     s3, p3, q3, z3, r3_ss, r3_rs,
-    hid, s2, p2, q2, z2, r2_ss, r2_rs,
+    hid, s2, p2, q2, z2, r2_ss, r2_rs, q_ss, q_rs,
     back, ret, b_ss, b_rs,
     hidden_ref,
 ):
@@ -220,8 +220,11 @@
     D = DT * tps
     cap = disp.shape[1]
 
-    def peer(k):
-        return me ^ k
+    def key(p):
+        return (p & 1) | ((p & 2) << 1) | ((p & 4) >> 1)
+
+    def peer(p):
+        return me ^ key(p)
 
     barrier = pltpu.get_barrier_semaphore()
     for k in range(1, n):
@@ -266,11 +269,9 @@
     last = jnp.max(doc, axis=1, keepdims=True)
     pool = pool_ref[...]
     tail_mask = jnp.broadcast_to((doc == last).astype(F32), (8, R))
-    stat_out[...] = jnp.zeros_like(stat_out)
-    stat_out[0:1, :] = dot(tail_mask.astype(BF16), pool)[0:1]
-    stat_out[1:2, :] = jnp.broadcast_to(last, (1, C))
-    stat_out[2:3, :] = jnp.broadcast_to(jnp.sum(tail_mask[0:1], axis=1, keepdims=True), (1, C))
-    stat_out[3:4, 0:R] = pltpu.roll(jnp.broadcast_to(doc, (8, R)), 16, axis=1)[0:1]
+    stat_out[:, 0:C] = dot(tail_mask.astype(BF16), pool)[0:1]
+    stat_out[:, C:C + 128] = jnp.broadcast_to(last, (1, 128))
+    stat_out[:, C + 128:C + 256] = jnp.broadcast_to(jnp.sum(tail_mask[0:1], axis=1, keepdims=True), (1, 128))
 
     t_pos = lax.broadcasted_iota(jnp.int32, (R, R), 0)
     u_pos = lax.broadcasted_iota(jnp.int32, (R, R), 1)
@@ -298,7 +299,7 @@
     totals.append(dot(same.astype(F32).astype(BF16), pool))
 
     e_iota = lax.broadcasted_iota(jnp.int32, (n, R), 0)
-    picked = (e_iota ^ me).astype(F32)
+    picked = (key(e_iota) ^ me).astype(F32)
     small[2].wait()
     routes = routes_ref[...].astype(F32)
     r0 = (jnp.broadcast_to(routes[0:1], (n, R)) == picked).astype(F32)
@@ -320,18 +321,19 @@
         arrived(stat_in.at[k], stat_ss.at[k], stat_rs.at[k], {"sp": peer(k)})
     carry = jnp.zeros((1, C), F32)
     carry_length = jnp.zeros((1, 1), F32)
-    before_doc = jnp.zeros((1, R), F32)
+    before = jnp.zeros((1, R), F32)
     for k in range(1, n):
-        source = jnp.full((1, C), peer(k), jnp.int32)
-        use = (stat_in[k, 1:2, :] == jnp.broadcast_to(first, (1, C))) & (source < me)
-        carry = carry + jnp.where(use, stat_in[k, 0:1, :], 0.0)
-        carry_length = carry_length + jnp.where(use, stat_in[k, 2:3, :], 0.0)[:, 0:1]
-        before_doc = before_doc + jnp.where(source[:, 0:R] == me - 1, stat_in[k, 3:4, 0:R], 0.0)
+        source = jnp.full((1, 128), peer(k), jnp.int32)
+        use = (stat_in[k, :, C:C + 128] == jnp.broadcast_to(first, (1, 128))) & (source < me)
+        tail = jnp.where(use, stat_in[k, :, C + 128:C + 256], 0.0)
+        keep = jnp.concatenate([use.astype(F32)] * (C // 128), axis=1)
+        carry = carry + keep * stat_in[k, :, 0:C]
+        carry_length = carry_length + tail[:, 0:1]
+        before = before + jnp.where(source == me - 1, tail, 0.0)
     in_first = (doc_col == first).astype(F32)[:, 0:1]
     length = length + in_first * carry_length
-    halo_doc = jnp.broadcast_to(before_doc, (R, R))
     reach = gap + 16
-    halo_ok = (halo_doc == doc_col) & (jnp.full((R, R), me, jnp.int32) > 0)
+    halo_ok = (doc_col == first) & (u_pos.astype(F32) >= 16.0 - jnp.broadcast_to(before, (R, R)))
     halo = jnp.where(jnp.full(halo_in.shape, me, jnp.int32) > 0, halo_in[...].astype(F32), 0.0).astype(BF16)
     totals = [
         total + dot((halo_ok & (reach < w)).astype(F32)[:, 0:16].astype(BF16), halo)
@@ -379,11 +381,13 @@
 
     send(normed_ref, xs.at[mt], xs_ss.at[0], xs_rs.at[0], {"tp": across})
     send(normed_ref, xs.at[mt], xs_ss.at[1], xs_rs.at[1], {"tp": mate})
-    for ps in (list(range(1, n // 2)), list(range(n // 2, n))):
-        span = slice(ps[0] * cap, (ps[-1] + 1) * cap)
-        disp[ps[0]:ps[-1] + 1] = dot(both[span, :], normed).astype(BF16).reshape(len(ps), cap, DT)
+    disp[1:n] = dot(both[cap:, :], normed).astype(BF16).reshape(n - 1, cap, DT)
+
+    def dispatch(*ps):
         for p in ps:
             send(disp.at[p], rows.at[p, mt], d_ss.at[p], d_rs.at[p], {"sp": peer(p)})
+
+    dispatch(1, 4, 5, 2, 3)
     xs[mt] = normed
 
     all_sq = sq_row[0:8]
@@ -399,9 +403,10 @@
     slot_scale = sum(
         lax.dot_general(part, both[...], turned, preferred_element_type=F32) for part in (high, middle, low))
     for p in range(n):
-        sc_out[p, :, 0:cap] = slot_scale[:, p * cap:(p + 1) * cap]
-        if p:
-            send(sc_out.at[p], sc_in.at[p], sc_ss.at[p], sc_rs.at[p], {"sp": peer(p)})
+        sc_out[p, :, 0:cap] = slot_scale[0:1, p * cap:(p + 1) * cap]
+    for p in (6, 7, 2, 3, 4, 5, 1):
+        send(sc_out.at[p], sc_in.at[p], sc_ss.at[p], sc_rs.at[p], {"sp": peer(p)})
+    dispatch(6, 7)
     scale = jnp.broadcast_to(scale_row[0:1], (R, R)).T[:, 0:1]
 
     def own_here(p):
@@ -469,7 +474,7 @@
         m = len(ps) * cap
         factors = []
         for p in ps:
-            line = (sc_in if p else sc_out)[p, 0:1, :]
+            line = (sc_in if p else sc_out)[p]
             factors.append(jnp.broadcast_to(line, (128, 128)).T[0:cap, 0:1])
         factor = jnp.concatenate(factors, 0)
         span = pl.ds(ps[0] * cap, m)
@@ -488,35 +493,43 @@
         lax.fori_loop(start, stop, up, 0)
 
     def expert_down(gi, half):
-        span = pl.ds(groups[gi][0] * cap, len(groups[gi]) * cap)
-        s, p, _, _, ss, rs = scatter_refs(gi)
+        span = span_of(gi)
 
         def down(j):
-            s[j] = dot(hid[span, :], ed[:, pl.ds(pl.multiple_of(j * DT, DT), DT)]).astype(BF16)
+            s2[j, span] = dot(hid[span, :], ed[:, pl.ds(pl.multiple_of(j * DT, DT), DT)]).astype(BF16)
 
         for i, y2 in enumerate((1 - yy, yy)):
             if i in half:
                 down(y2 * 2 + 1 - core)
-                send(s.at[y2 * 2 + 1 - core], p.at[i], ss.at[i], rs.at[i], {"tp": mate})
+                send(s2.at[y2 * 2 + 1 - core, span], p2.at[i, span], r2_ss.at[gi, i], r2_rs.at[gi, i], {"tp": mate})
                 down(y2 * 2 + core)
 
-    def scatter_refs(gi):
-        span = pl.ds(groups[gi][0] * cap, len(groups[gi]) * cap)
-        return (s2.at[:, span], p2.at[:, span], q2.at[span], z2.at[span], r2_ss.at[gi], r2_rs.at[gi])
-
-    def across2(gi):
-        scatter_across(*scatter_refs(gi))
-
-    def give_back(gi):
-        s, p, q, z, ss, rs = scatter_refs(gi)
-        total = scatter_end(s, p, z, ss, rs).astype(BF16)
-        for i, p in enumerate(groups[gi]):
-            piece = total[i * cap:(i + 1) * cap]
+    def span_of(gi):
+        return pl.ds(groups[gi][0] * cap, len(groups[gi]) * cap)
+
+    def scatter_sum(gi):
+        span = span_of(gi)
+        arrived(p2.at[0, span], r2_ss.at[gi, 0], r2_rs.at[gi, 0], {"tp": mate})
+        q2[span] = (s2[across, span].astype(F32) + p2[0, span].astype(F32)).astype(BF16)
+
+    def scatter_send(*ps):
+        for p in ps:
+            piece = pl.ds(p * cap, cap)
+            send(q2.at[piece], z2.at[piece], q_ss.at[p], q_rs.at[p], {"tp": across})
+
+    def mate_sum(gi):
+        arrived(p2.at[1, span_of(gi)], r2_ss.at[gi, 1], r2_rs.at[gi, 1], {"tp": mate})
+
+    def give_back(*ps):
+        for p in ps:
+            piece = pl.ds(p * cap, cap)
+            arrived(z2.at[piece], q_ss.at[p], q_rs.at[p], {"tp": across})
+            total = (s2[mt, piece].astype(F32) + p2[1, piece].astype(F32) + z2[piece].astype(F32)).astype(BF16)
             if p == 0:
-                ret[0:cap, :] = piece
+                ret[piece] = total
             else:
-                back[p] = piece
-                send(back.at[p], ret.at[pl.ds(p * cap, cap)], b_ss.at[p], b_rs.at[p], {"sp": peer(p)})
+                back[p] = total
+                send(back.at[p], ret.at[piece], b_ss.at[p], b_rs.at[p], {"sp": peer(p)})
 
     def collect(gi):
         span = pl.ds(groups[gi][0] * cap, len(groups[gi]) * cap)
@@ -534,50 +547,61 @@
     forward_own(1)
     xs_across()
     forward_own(2)
-    forward_own(4)
     forward_across(1)
     xs_rest()
-    forward_own(5)
+    forward_own(3)
     weights_here()
     all_here(0, 1)
     expert_up(0, 0, 2)
-    forward_own(3)
-    forward_across(2, 4)
+    forward_across(2)
+    forward_own(4, 5)
     expert_up(0, 2, 4)
+    expert_down(0, (0,))
+    forward_own(6)
+    expert_down(0, (1,))
+    forward_across(3)
+    shared()
+    all_here(2, 3)
+    expert_up(1, 0, 2)
+    forward_own(7)
+    forward_across(4)
+    expert_up(1, 2, 4)
     forward_across(5)
-    forward_own(6)
-    expert_down(0, (0,))
-    forward_across(3)
-    expert_down(0, (1,))
-    forward_own(7)
+    expert_down(1, (0, 1))
     all_here(4, 5)
-    expert_up(2, 0, 2)
+    expert_up(2, 0, 1)
+    scatter_sum(1)
+    scatter_send(2, 3)
     forward_across(6)
-    across2(0)
-    expert_up(2, 2, 4)
-    expert_down(2, (0, 1))
+    expert_up(2, 1, 2)
     forward_across(7)
-    shared()
-    across2(2)
+    scatter_sum(0)
+    scatter_send(1, 0)
+    expert_up(2, 2, 3)
     all_here(6, 7)
     expert_up(3)
-    give_back(0)
+    mate_sum(1)
+    give_back(2)
     expert_down(3, (0, 1))
-    all_here(2, 3)
-    expert_up(1, 0, 2)
-    across2(3)
-    give_back(2)
-    expert_up(1, 2, 4)
-    expert_down(1, (0, 1))
+    give_back(3)
+    expert_up(2, 3, 4)
+    scatter_sum(3)
+    scatter_send(6, 7)
+    expert_down(2, (0, 1))
+    mate_sum(0)
+    give_back(1)
+    scatter_sum(2)
+    scatter_send(4, 5)
+    shared_across()
+    mate_sum(3)
+    give_back(6, 7)
+    mate_sum(2)
+    give_back(4, 5, 0)
     collect(0)
-    give_back(3)
-    across2(1)
-    shared_across()
-    collect(2)
-    give_back(1)
+    collect(1)
     shared_end()
     collect(3)
-    collect(1)
+    collect(2)
     out_ref[...] = hidden_ref[...].astype(BF16)
     for copy in sends:
         copy.wait_send()
@@ -608,16 +632,16 @@
         V((R, DT), BF16), V((1, C), F32), V((1, DT), F32), DMA((7,)),
         V((C, D), BF16), V((D, FF), BF16), V((D, FF), BF16), V((FF, D), BF16),
         V((D, FS), BF16), V((D, FS), BF16), V((FS, D), BF16), DMA((7,)),
-        V((8, C), F32), V((n, 8, C), F32), V((16, C), BF16), DMA((n,)), DMA((n,)), DMA((2,)),
+        V((1, C + 256), F32), V((n, 1, C + 256), F32), V((16, C), BF16), DMA((n,)), DMA((n,)), DMA((2,)),
         V((tps, R, DT), BF16), V((2, R, DT), BF16), V((R, DT), BF16), V((R, DT), BF16), DMA((3,)), DMA((3,)),
         V((8, R), F32), V((tps, 8, R), F32), DMA((tps,)), DMA((tps,)),
-        V((2, n * cap, R), BF16), V((n * cap, R), BF16), V((n, 8, 128), F32), V((n, 8, 128), F32), DMA((n,)), DMA((n,)),
+        V((2, n * cap, R), BF16), V((n * cap, R), BF16), V((n, 1, 128), F32), V((n, 1, 128), F32), DMA((n,)), DMA((n,)),
         V((n, cap, DT), BF16), V((n, tps, cap, DT), BF16),
         DMA((n,)), DMA((n,)), DMA((n, 3)), DMA((n, 3)),
         V((R, DT), BF16), V((tps, R, DT), BF16), DMA((3,)), DMA((3,)),
         V((tps, R, DT), BF16), V((2, R, DT), BF16), V((R, DT), BF16), V((R, DT), BF16), DMA((3,)), DMA((3,)),
         V((n * cap, FF), BF16), V((tps, n * cap, DT), BF16), V((2, n * cap, DT), BF16),
-        V((n * cap, DT), BF16), V((n * cap, DT), BF16), DMA((len(groups), 3)), DMA((len(groups), 3)),
+        V((n * cap, DT), BF16), V((n * cap, DT), BF16), DMA((len(groups), 2)), DMA((len(groups), 2)), DMA((n,)), DMA((n,)),
         V((n, cap, DT), BF16), V((n * cap, DT), BF16), DMA((n,)), DMA((n,)),
         V((R, DT), F32),
     ]

time: 59.3 us -> 56.5 us (0.953)
  Pallas kernels: 57.5 us -> 54.7 us
    pallas_call x1, Pallas kernels: 57.5 us -> 54.7 us  [body(): pl.pallas_call(functools.partial(layer_kernel, groups), out_shape=jax.Sha...]
where the time goes in v2:
time: 56.5 us; the launch traced here: 56.3 us
  Pallas kernels  54.7 us (97%)
  local copies, waits for them, and re-layouts  1.57 us (3%)
    pallas_call x1, Pallas kernels, body(): pl.pallas_call(functools.partial(layer_kernel, groups), out_shape=jax.Sha...  54.7 us
    unnamed x1, local copies, waits for them, and re-layouts  1.57 us

profile of v2, /device:TPU:0, one launch (start us, length us, event | category | flops | bytes accessed | tf_op | source)
XLA Modules:
  0.0 56.3 jit_solution(1068152174482072545)
XLA Ops:
  0.0 54.7 %shard_map.136 = bf16[128,512]{1,0:T(8,128)(2,1)} custom-call(bf16[128,256]{1,0:T(8,128)(2,1)} %pool_hbm.1, s32[1,128]{1,0:T(1,128)} %bitcast.9, s32[2,128]{1,0:T(2,128)} %bitcast.6, f32[2,128]{1,0:T(2,128)} %bitcast.7, bf16[128,512]{1,0:T(8,128)(2,1)} %resid_hbm.1, f32[1,256]{1,0:T(1,128)} %bitcast.8, f32[1,512]{1,0:T(1,128)} %bitcast.5, ...), custom_call_target="tpu_custom_call" | custom-call | tf_op jit(solution)/shard_map/pallas_call | solution.py:650
  54.8 1.6 %copy.16 = bf16[128,512]{1,0:T(8,128)(2,1)} copy(bf16[128,512]{1,0:T(8,128)(2,1)} %shard_map.136) | data formatting | bytes 262144

commit v3 on v2

--- a/solution.py
+++ b/solution.py
@@ -365,30 +365,44 @@
     for j in range(tps):
         s1[j] = dot(pooled, oproj[:, j * DT:(j + 1) * DT]).astype(BF16)
     scatter_start(s1, p1, r1_ss, r1_rs)
-    scatter_across(s1, p1, q1, z1, r1_ss, r1_rs)
-    projected = scatter_end(s1, p1, z1, r1_ss, r1_rs)
+    halves = [slice(h * DT // 2, (h + 1) * DT // 2) for h in range(2)]
+    arrived(p1.at[0], r1_ss.at[0], r1_rs.at[0], {"tp": mate})
+    q1[...] = (s1[across].astype(F32) + p1[0].astype(F32)).astype(BF16)
+    for h, part in enumerate(halves):
+        send(q1.at[:, part], z1.at[:, part], r1_ss.at[2 + h], r1_rs.at[2 + h], {"tp": across})
     for load in small[4:]:
         load.wait()
-    hidden = resid_ref[...].astype(F32) + projected
-    hidden_ref[...] = hidden
-    squares = jnp.sum(hidden * hidden, axis=1, keepdims=True)
-    sq_row = jnp.broadcast_to(squares, (R, R)).T
-    ss_out[...] = sq_row[0:8]
-    for j in range(1, tps):
-        send(ss_out, ss_in.at[j], ss_ss.at[j], ss_rs.at[j], {"tp": lax.rem(mt + j, tps)})
-    normed = (hidden * ngain_ref[...]).astype(BF16)
-    normed_ref[...] = normed
-
-    send(normed_ref, xs.at[mt], xs_ss.at[0], xs_rs.at[0], {"tp": across})
-    send(normed_ref, xs.at[mt], xs_ss.at[1], xs_rs.at[1], {"tp": mate})
-    disp[1:n] = dot(both[cap:, :], normed).astype(BF16).reshape(n - 1, cap, DT)
+    arrived(p1.at[1], r1_ss.at[1], r1_rs.at[1], {"tp": mate})
+    hidden_ref[...] = resid_ref[...].astype(F32) + (s1[mt].astype(F32) + p1[1].astype(F32))
+
+    def gather(p, count, part):
+        slots = dot(both[p * cap:(p + count) * cap, :], normed_ref[:, part]).astype(BF16)
+        disp[p:p + count, :, part] = slots.reshape(count, cap, slots.shape[1])
 
     def dispatch(*ps):
         for p in ps:
-            send(disp.at[p], rows.at[p, mt], d_ss.at[p], d_rs.at[p], {"sp": peer(p)})
-
-    dispatch(1, 4, 5, 2, 3)
-    xs[mt] = normed
+            send(disp.at[p], rows.at[p, mt], d_ss.at[p, 0], d_rs.at[p, 0], {"sp": peer(p)})
+
+    partial = []
+    for h, part in enumerate(halves):
+        arrived(z1.at[:, part], r1_ss.at[2 + h], r1_rs.at[2 + h], {"tp": across})
+        hidden = hidden_ref[:, part] + z1[:, part].astype(F32)
+        normed_ref[:, part] = (hidden * ngain_ref[:, part]).astype(BF16)
+        gather(1, 5, part)
+        for p in (4, 5, 2, 3, 1):
+            send(disp.at[p, :, part], rows.at[p, mt, :, part], d_ss.at[p, h], d_rs.at[p, h], {"sp": peer(p)})
+        hidden_ref[:, part] = hidden
+        partial.append(jnp.sum(hidden * hidden, axis=1, keepdims=True))
+        if h:
+            sq_row = jnp.broadcast_to(partial[0] + partial[1], (R, R)).T
+            ss_out[...] = sq_row[0:8]
+            for j in range(1, tps):
+                send(ss_out, ss_in.at[j], ss_ss.at[j], ss_rs.at[j], {"tp": lax.rem(mt + j, tps)})
+        send(normed_ref.at[:, part], xs.at[mt, :, part], xs_ss.at[3 * h], xs_rs.at[3 * h], {"tp": across})
+        send(normed_ref.at[:, part], xs.at[mt, :, part], xs_ss.at[3 * h + 1], xs_rs.at[3 * h + 1], {"tp": mate})
+    gather(6, 2, slice(0, DT))
+    dispatch(6)
+    xs[mt] = normed_ref[...]
 
     all_sq = sq_row[0:8]
     for j in range(1, tps):
@@ -406,20 +420,19 @@
         sc_out[p, :, 0:cap] = slot_scale[0:1, p * cap:(p + 1) * cap]
     for p in (6, 7, 2, 3, 4, 5, 1):
         send(sc_out.at[p], sc_in.at[p], sc_ss.at[p], sc_rs.at[p], {"sp": peer(p)})
-    dispatch(6, 7)
+    dispatch(7)
     scale = jnp.broadcast_to(scale_row[0:1], (R, R)).T[:, 0:1]
 
     def own_here(p):
-        arrived(rows.at[p, mt], d_ss.at[p], d_rs.at[p], {"sp": peer(p)})
+        if p < 6:
+            for h, part in enumerate(halves):
+                arrived(rows.at[p, mt, :, part], d_ss.at[p, h], d_rs.at[p, h], {"sp": peer(p)})
+        else:
+            arrived(rows.at[p, mt], d_ss.at[p, 0], d_rs.at[p, 0], {"sp": peer(p)})
 
     def forward_own(*ps):
         for p in ps:
             own_here(p)
-            send(rows.at[p, mt], rows.at[p, mt], ag_ss.at[p, 0], ag_rs.at[p, 0], {"tp": across})
-            send(rows.at[p, mt], rows.at[p, mt], ag_ss.at[p, 1], ag_rs.at[p, 1], {"tp": mate})
-
-    def forward_own2(*ps):
-        for p in ps:
             send(rows.at[p, mt], rows.at[p, mt], ag_ss.at[p, 0], ag_rs.at[p, 0], {"tp": across})
             send(rows.at[p, mt], rows.at[p, mt], ag_ss.at[p, 1], ag_rs.at[p, 1], {"tp": mate})
 
@@ -436,11 +449,13 @@
                 arrived(sc_in.at[p], sc_ss.at[p], sc_rs.at[p], {"sp": peer(p)})
 
     def xs_across():
-        arrived(xs.at[across], xs_ss.at[0], xs_rs.at[0], {"tp": across})
+        for h, part in enumerate(halves):
+            arrived(xs.at[across, :, part], xs_ss.at[3 * h], xs_rs.at[3 * h], {"tp": across})
         send(xs.at[across], xs.at[across], xs_ss.at[2], xs_rs.at[2], {"tp": mate})
 
     def xs_rest():
-        arrived(xs.at[mate], xs_ss.at[1], xs_rs.at[1], {"tp": mate})
+        for h, part in enumerate(halves):
+            arrived(xs.at[mate, :, part], xs_ss.at[3 * h + 1], xs_rs.at[3 * h + 1], {"tp": mate})
         arrived(xs.at[(1 - yy) * 2 + 1 - core], xs_ss.at[2], xs_rs.at[2], {"tp": mate})
         for j in range(tps):
             rows[0, j] = dot(both[0:cap, :], xs[j]).astype(BF16)
@@ -455,15 +470,19 @@
         g = sum(dot(xs[j], sg[j * DT:(j + 1) * DT, :]) for j in range(tps)) * scale
         u = sum(dot(xs[j], su[j * DT:(j + 1) * DT, :]) for j in range(tps)) * scale
         hs = (silu(g) * u).astype(BF16)
+        own = weights_ref[0:1, :] * r0[0:1] + weights_ref[1:2, :] * r1[0:1]
+        own = jnp.broadcast_to(own, (R, R)).T[:, 0:1]
         for j in range(tps):
-            s3[j] = dot(hs, sd[:, j * DT:(j + 1) * DT]).astype(BF16)
+            routed = lax.dot_general(
+                both[0:cap, :], s2[j, 0:cap], (((0,), (0,)), ((), ())), preferred_element_type=F32)
+            s3[j] = (dot(hs, sd[:, j * DT:(j + 1) * DT]) + own * routed).astype(BF16)
         scatter_start(s3, p3, r3_ss, r3_rs)
 
     def shared_across():
         scatter_across(s3, p3, q3, z3, r3_ss, r3_rs)
 
     def shared_end():
-        hidden_ref[...] = hidden_ref[...] + scatter_end(s3, p3, z3, r3_ss, r3_rs).astype(BF16).astype(F32)
+        hidden_ref[...] = hidden_ref[...] + scatter_end(s3, p3, z3, r3_ss, r3_rs)
 
     FF = eg.shape[1]
     tile = 256 if FF % 256 == 0 else FF
@@ -494,9 +513,10 @@
 
     def expert_down(gi, half):
         span = span_of(gi)
+        whole = pl.ds(groups[gi][0] * cap, len(groups[gi]) * cap)
 
         def down(j):
-            s2[j, span] = dot(hid[span, :], ed[:, pl.ds(pl.multiple_of(j * DT, DT), DT)]).astype(BF16)
+            s2[j, whole] = dot(hid[whole, :], ed[:, pl.ds(pl.multiple_of(j * DT, DT), DT)]).astype(BF16)
 
         for i, y2 in enumerate((1 - yy, yy)):
             if i in half:
@@ -505,7 +525,8 @@
                 down(y2 * 2 + core)
 
     def span_of(gi):
-        return pl.ds(groups[gi][0] * cap, len(groups[gi]) * cap)
+        away = [p for p in groups[gi] if p]
+        return pl.ds(away[0] * cap, len(away) * cap)
 
     def scatter_sum(gi):
         span = span_of(gi)
@@ -525,14 +546,11 @@
             piece = pl.ds(p * cap, cap)
             arrived(z2.at[piece], q_ss.at[p], q_rs.at[p], {"tp": across})
             total = (s2[mt, piece].astype(F32) + p2[1, piece].astype(F32) + z2[piece].astype(F32)).astype(BF16)
-            if p == 0:
-                ret[piece] = total
-            else:
-                back[p] = total
-                send(back.at[p], ret.at[piece], b_ss.at[p], b_rs.at[p], {"sp": peer(p)})
+            back[p] = total
+            send(back.at[p], ret.at[piece], b_ss.at[p], b_rs.at[p], {"sp": peer(p)})
 
     def collect(gi):
-        span = pl.ds(groups[gi][0] * cap, len(groups[gi]) * cap)
+        span = span_of(gi)
         for p in groups[gi]:
             if p:
                 arrived(ret.at[pl.ds(p * cap, cap)], b_ss.at[p], b_rs.at[p], {"sp": peer(p)})
@@ -561,42 +579,39 @@
     expert_down(0, (1,))
     forward_across(3)
     shared()
+    forward_own(7)
     all_here(2, 3)
     expert_up(1, 0, 2)
-    forward_own(7)
     forward_across(4)
     expert_up(1, 2, 4)
     forward_across(5)
     expert_down(1, (0, 1))
-    all_here(4, 5)
-    expert_up(2, 0, 1)
     scatter_sum(1)
     scatter_send(2, 3)
-    forward_across(6)
-    expert_up(2, 1, 2)
-    forward_across(7)
     scatter_sum(0)
-    scatter_send(1, 0)
-    expert_up(2, 2, 3)
+    scatter_send(1)
+    forward_across(6, 7)
+    all_here(4, 5)
+    expert_up(2, 0, 2)
     all_here(6, 7)
     expert_up(3)
     mate_sum(1)
     give_back(2)
     expert_down(3, (0, 1))
-    give_back(3)
-    expert_up(2, 3, 4)
     scatter_sum(3)
     scatter_send(6, 7)
+    give_back(3)
+    expert_up(2, 2, 4)
     expert_down(2, (0, 1))
     mate_sum(0)
     give_back(1)
+    mate_sum(3)
     scatter_sum(2)
     scatter_send(4, 5)
     shared_across()
-    mate_sum(3)
     give_back(6, 7)
     mate_sum(2)
-    give_back(4, 5, 0)
+    give_back(4, 5)
     collect(0)
     collect(1)
     shared_end()
@@ -633,12 +648,12 @@
         V((C, D), BF16), V((D, FF), BF16), V((D, FF), BF16), V((FF, D), BF16),
         V((D, FS), BF16), V((D, FS), BF16), V((FS, D), BF16), DMA((7,)),
         V((1, C + 256), F32), V((n, 1, C + 256), F32), V((16, C), BF16), DMA((n,)), DMA((n,)), DMA((2,)),
-        V((tps, R, DT), BF16), V((2, R, DT), BF16), V((R, DT), BF16), V((R, DT), BF16), DMA((3,)), DMA((3,)),
+        V((tps, R, DT), BF16), V((2, R, DT), BF16), V((R, DT), BF16), V((R, DT), BF16), DMA((4,)), DMA((4,)),
         V((8, R), F32), V((tps, 8, R), F32), DMA((tps,)), DMA((tps,)),
         V((2, n * cap, R), BF16), V((n * cap, R), BF16), V((n, 1, 128), F32), V((n, 1, 128), F32), DMA((n,)), DMA((n,)),
         V((n, cap, DT), BF16), V((n, tps, cap, DT), BF16),
-        DMA((n,)), DMA((n,)), DMA((n, 3)), DMA((n, 3)),
-        V((R, DT), BF16), V((tps, R, DT), BF16), DMA((3,)), DMA((3,)),
+        DMA((n, 2)), DMA((n, 2)), DMA((n, 3)), DMA((n, 3)),
+        V((R, DT), BF16), V((tps, R, DT), BF16), DMA((5,)), DMA((5,)),
         V((tps, R, DT), BF16), V((2, R, DT), BF16), V((R, DT), BF16), V((R, DT), BF16), DMA((3,)), DMA((3,)),
         V((n * cap, FF), BF16), V((tps, n * cap, DT), BF16), V((2, n * cap, DT), BF16),
         V((n * cap, DT), BF16), V((n * cap, DT), BF16), DMA((len(groups), 2)), DMA((len(groups), 2)), DMA((n,)), DMA((n,)),
@@ -649,7 +664,7 @@
     hb = pl.BlockSpec(memory_space=pltpu.HBM)
     return pl.pallas_call(
         functools.partial(layer_kernel, groups),
-        out_shape=jax.ShapeDtypeStruct((R, DT), BF16),
+        out_shape=pltpu.VMEM((R, DT), BF16),
         in_specs=[hb] * 14,
         out_specs=vm,
         scratch_shapes=scratch,

time: 56.5 us -> 53 us (0.938)
  Pallas kernels: 54.7 us -> 52.2 us
  local copies, waits for them, and re-layouts: 1.57 us -> 0.66 us
    pallas_call x1, Pallas kernels: 54.7 us -> 52.2 us  [body(): pl.pallas_call(functools.partial(layer_kernel, groups), out_shape=pltpu.V...]
    unnamed x1, local copies, waits for them, and re-layouts: 1.57 us -> 0.66 us
where the time goes in v3:
time: 53 us; the launch traced here: 52.8 us
  Pallas kernels  52.2 us (98%)
  local copies, waits for them, and re-layouts  0.66 us (1%)
    pallas_call x1, Pallas kernels, body(): pl.pallas_call(functools.partial(layer_kernel, groups), out_shape=pltpu.V...  52.2 us

profile of v3, /device:TPU:0, one launch (start us, length us, event | category | flops | bytes accessed | tf_op | source)
XLA Modules:
  0.0 52.8 jit_solution(3610012742577073405)
XLA Ops:
  0.0 52.2 %shard_map.136 = bf16[128,512]{1,0:T(8,128)(2,1)S(1)} custom-call(bf16[128,256]{1,0:T(8,128)(2,1)} %pool_hbm.1, s32[1,128]{1,0:T(1,128)} %bitcast.9, s32[2,128]{1,0:T(2,128)} %bitcast.6, f32[2,128]{1,0:T(2,128)} %bitcast.7, bf16[128,512]{1,0:T(8,128)(2,1)} %resid_hbm.1, f32[1,256]{1,0:T(1,128)} %bitcast.8, f32[1,512]{1,0:T(1,128)} %bitcast.5, ...), custom_call_target="tpu_custom_call" | custom-call | tf_op jit(solution)/shard_map/pallas_call | solution.py:665
  52.2 0.7 %copy.16 = bf16[128,512]{1,0:T(8,128)(2,1)} copy(bf16[128,512]{1,0:T(8,128)(2,1)S(1)} %shard_map.136) | data formatting | bytes 262144

commit v4 on v3

--- a/solution.py
+++ b/solution.py
@@ -389,7 +389,7 @@
         hidden = hidden_ref[:, part] + z1[:, part].astype(F32)
         normed_ref[:, part] = (hidden * ngain_ref[:, part]).astype(BF16)
         gather(1, 5, part)
-        for p in (4, 5, 2, 3, 1):
+        for p in (1, 2, 4, 3, 5):
             send(disp.at[p, :, part], rows.at[p, mt, :, part], d_ss.at[p, h], d_rs.at[p, h], {"sp": peer(p)})
         hidden_ref[:, part] = hidden
         partial.append(jnp.sum(hidden * hidden, axis=1, keepdims=True))

time: 53 us -> 52.8 us (level)
  no operation moved by 1% of the time
where the time goes in v4:
time: 52.8 us; the launch traced here: 52.6 us
  Pallas kernels  52 us (98%)
  local copies, waits for them, and re-layouts  0.66 us (1%)
    pallas_call x1, Pallas kernels, body(): pl.pallas_call(functools.partial(layer_kernel, groups), out_shape=pltpu.V...  52 us

profile of v4, /device:TPU:0, one launch (start us, length us, event | category | flops | bytes accessed | tf_op | source)
XLA Modules:
  0.0 52.6 jit_solution(12251629628670800391)
XLA Ops:
  0.0 52.0 %shard_map.136 = bf16[128,512]{1,0:T(8,128)(2,1)S(1)} custom-call(bf16[128,256]{1,0:T(8,128)(2,1)} %pool_hbm.1, s32[1,128]{1,0:T(1,128)} %bitcast.9, s32[2,128]{1,0:T(2,128)} %bitcast.6, f32[2,128]{1,0:T(2,128)} %bitcast.7, bf16[128,512]{1,0:T(8,128)(2,1)} %resid_hbm.1, f32[1,256]{1,0:T(1,128)} %bitcast.8, f32[1,512]{1,0:T(1,128)} %bitcast.5, ...), custom_call_target="tpu_custom_call" | custom-call | tf_op jit(solution)/shard_map/pallas_call | solution.py:665
  52.0 0.7 %copy.16 = bf16[128,512]{1,0:T(8,128)(2,1)} copy(bf16[128,512]{1,0:T(8,128)(2,1)S(1)} %shard_map.136) | data formatting | bytes 262144
